TPU v7x, 32 devices: a whole 2x2x4 slice. The times are simulated.
32 devices in a mesh: ep: 8 (over z, y), tp: 4 (over x, core).
Axes of the slice: x: 2, y: 2, z: 4, core: 2. Of those that a mesh axis runs over, the one named last changes fastest.
Arguments:
- glu_value: bfloat16 [4096, 1024], P('ep', 'tp'), may hold values from -6 to 6
- glu_gate: bfloat16 [4096, 1024], P('ep', 'tp'), may hold values from -12 to 12
- conv_kernel: float32 [31, 1024], P(None, 'tp'), may hold values from -11.49474 to 11.49474
- ln_gain: float32 [1024], P('tp'), may hold values from 0.1 to 1.9
- out_weight: bfloat16 [1024, 2048], P('tp'), may hold values from -0.1875 to 0.1875
- moe_input: bfloat16 [2048, 2048], P('ep'), may hold values from -6 to 6
- moe_gain: float32 [2048], replicated, may hold values from 0.1 to 1.9
- gate_weight: bfloat16 [8, 2048, 3072], P('ep', None, 'tp'), may hold values from -0.125 to 0.125
- up_weight: bfloat16 [8, 2048, 3072], P('ep', None, 'tp'), may hold values from -0.125 to 0.125
- down_weight: bfloat16 [8, 3072, 2048], P('ep', 'tp'), may hold values from -0.109375 to 0.109375
- expert_ids: int32 [2048, 2], P('ep'), may hold values from 0 to 7, all different within a row; in each aligned block of 256 rows (0 to 255, 256 to 511, ...) at most 128 rows name the same one
- route_weight: float32 [2048, 2], P('ep'), may hold values from 0.2 to 1
Outputs:
- mixer_out: bfloat16 [4096, 2048], P(('ep', 'tp'))
- expert_out: bfloat16 [2048, 2048], P('ep', 'tp')
Inputs may be any that keep to these rules, and one draw needn't show every extreme that they name: `expert_ids`: each row names 2 different experts. In the rows of one device no expert is named by more than 128 rows; the bound is reached at some expert in some device's rows.
All inputs are finite; a program needn't handle non-finite values.
Results may differ from a plain program's by a relative error of at most 0.012.
Values may be sent and summed in bfloat16 or wider, within the bound.
A program may use at most 64 MiB of HBM per device.

v0:
```python
import functools

import jax
import jax.numpy as jnp
from jax import lax
from jax.experimental import pallas as pl
from jax.experimental.pallas import tpu as pltpu
from jax.sharding import PartitionSpec as P

eps_rms = 1e-06
eps_norm = 1e-05
MESH = pl.DeviceIdType.MESH
f32 = jnp.float32
bf16 = jnp.bfloat16


def kernel(
    n,
    tp,
    cap,
    group,
    reach,
    moe_ref,
    moe_gain_ref,
    ids_ref,
    ids_t_ref,
    route_ref,
    taps_ref,
    ln_gain_ref,
    value_hbm,
    gate_hbm,
    w_out_hbm,
    w_gate_hbm,
    w_up_hbm,
    w_down_hbm,
    mixer_ref,
    expert_ref,
    value,
    gate,
    w_out,
    w_gate,
    w_up,
    w_down,
    load_sem,
    normed,
    slots,
    near_slots,
    onehots,
    arrived,
    near_send,
    near_recv,
    fn_send,
    fn_recv,
    a2a_send,
    a2a_recv,
    fx_send,
    fx_recv,
    fp_send,
    fp_recv,
    fq_send,
    fq_recv,
    gated,
    halo_in,
    halo_send,
    halo_recv,
    padded,
    conv,
    stat_out,
    stat_in,
    stat_send,
    stat_recv,
    act,
    mix_out,
    mix_own,
    mix_in,
    mix_send,
    mix_recv,
    mix_x_out,
    mix_x_in,
    mix_x_send,
    mix_x_recv,
    rs_out,
    rs_own,
    rs_in,
    rs_send,
    rs_recv,
    rx_out,
    rx_in,
    rx_send,
    rx_recv,
    answer,
    returned,
    ret_send,
    ret_recv,
    total,
):
    me = lax.axis_index("ep")
    mine = lax.axis_index("tp")
    core = lax.rem(mine, 2)
    chip = mine // 2
    partner = chip * 2 + 1 - core
    chips = tp // 2
    groups = n // group
    rows = group * cap
    tokens, width = moe_ref.shape
    quarter = width // tp
    length, chan = value.shape
    halo = halo_in.shape[0]
    own_rows = length // tp

    def toward(k):
        return lax.rem(me // 2 + k // 2, n // 2) * 2 + lax.rem(me + k, 2)

    def source(k):
        return lax.rem(me // 2 + n // 2 - k // 2, n // 2) * 2 + lax.rem(me + k, 2)

    def block(k):
        return pl.ds(pl.multiple_of(k * cap, cap), cap)

    def columns_of(part):
        return pl.ds(pl.multiple_of(part * quarter, 128), quarter)

    def across(j):
        there = lax.rem(chip + j, chips)
        here = lax.rem(chip + chips - j, chips)
        return there * 2 + core, here * 2 + core

    barrier = pltpu.get_barrier_semaphore()

    def greet_ep(k, _):
        pl.semaphore_signal(
            barrier, inc=1, device_id={"ep": lax.rem(me + k, n)}, device_id_type=MESH
        )
        return 0

    lax.fori_loop(1, n, greet_ep, 0)
    for j in range(1, tp):
        pl.semaphore_signal(
            barrier, inc=1, device_id={"tp": lax.rem(mine + j, tp)}, device_id_type=MESH
        )

    loads = [
        pltpu.make_async_copy(src, dst, load_sem.at[i])
        for i, (src, dst) in enumerate(
            [
                (value_hbm, value),
                (gate_hbm, gate),
                (w_out_hbm, w_out),
                (w_gate_hbm.at[0], w_gate),
                (w_up_hbm.at[0], w_up),
                (w_down_hbm.at[0], w_down),
            ]
        )
    ]
    for load in loads:
        load.start()

    everything = moe_ref[...].astype(f32)
    inverse = lax.rsqrt(jnp.sum(everything * everything, axis=1, keepdims=True) / width + eps_rms)
    normed[...] = (everything * inverse * moe_gain_ref[...]).astype(bf16)
    row = lax.broadcasted_iota(jnp.int32, (tokens, tokens), 0)
    col = lax.broadcasted_iota(jnp.int32, (tokens, tokens), 1)
    below = (col < row).astype(f32).astype(bf16)
    above = (row < col).astype(f32).astype(bf16)

    def a2a_copy(k):
        return pltpu.make_async_remote_copy(
            src_ref=slots.at[block(k)],
            dst_ref=arrived.at[mine, block(k)],
            send_sem=a2a_send.at[k],
            recv_sem=a2a_recv.at[k],
            device_id={"ep": toward(k)},
            device_id_type=MESH,
        )

    def near_copy(xx):
        return pltpu.make_async_remote_copy(
            src_ref=near_slots.at[xx],
            dst_ref=arrived.at[xx * 2 + core, pl.ds(cap, cap)],
            send_sem=near_send.at[xx],
            recv_sem=near_recv.at[xx],
            device_id={"ep": toward(1)},
            device_id_type=MESH,
        )

    def slot_picks(k):
        expert = toward(k)
        member = jnp.maximum(
            (ids_t_ref[0:1, :] == expert).astype(f32), (ids_t_ref[1:2, :] == expert).astype(f32)
        )
        member = jnp.broadcast_to(member, (cap, tokens))
        place = jnp.dot(member.astype(bf16), above, preferred_element_type=f32)
        slot = lax.broadcasted_iota(jnp.int32, (cap, tokens), 0).astype(f32)
        return jnp.where(place == slot, member, 0.0).astype(bf16)

    def picked(pick, part):
        return jnp.dot(
            pick, normed[:, columns_of(part)], preferred_element_type=f32
        ).astype(bf16)

    pl.semaphore_wait(barrier, n - 1 + tp - 1)

    def dispatch(k, _):
        slots[block(k), :] = picked(slot_picks(k), mine)
        a2a_copy(k).start()
        return 0

    lax.fori_loop(2, n, dispatch, 0)
    pick = slot_picks(1)
    for xx in range(chips):
        near_slots[xx] = picked(pick, xx * 2 + core)
        near_copy(xx).start()

    loads[0].wait()
    loads[1].wait()
    gated_now = (value[...].astype(f32) * jax.nn.sigmoid(gate[...].astype(f32))).astype(bf16)
    gated[...] = gated_now
    halo_copy = pltpu.make_async_remote_copy(
        src_ref=gated.at[pl.ds(length - halo, halo)],
        dst_ref=halo_in,
        send_sem=halo_send,
        recv_sem=halo_recv,
        device_id={"ep": lax.rem(me + 1, n)},
        device_id_type=MESH,
    )
    halo_copy.start()
    padded[pl.ds(halo, length), :] = gated_now.astype(f32)

    pick = slot_picks(0)
    for part in range(tp):
        arrived[part, 0:cap, :] = picked(pick, part)

    def fx_copy(k, j):
        to, _ = across(j)
        return pltpu.make_async_remote_copy(
            src_ref=arrived.at[mine, block(k)],
            dst_ref=arrived.at[mine, block(k)],
            send_sem=fx_send.at[k, j - 1],
            recv_sem=fx_recv.at[k, j - 1],
            device_id={"tp": to},
            device_id_type=MESH,
        )

    def fp_copy(k):
        return pltpu.make_async_remote_copy(
            src_ref=arrived.at[mine, block(k)],
            dst_ref=arrived.at[mine, block(k)],
            send_sem=fp_send.at[k],
            recv_sem=fp_recv.at[k],
            device_id={"tp": partner},
            device_id_type=MESH,
        )

    def fq_copy(k, j):
        _, origin = across(j)
        return pltpu.make_async_remote_copy(
            src_ref=arrived.at[origin, block(k)],
            dst_ref=arrived.at[origin, block(k)],
            send_sem=fq_send.at[k, j - 1],
            recv_sem=fq_recv.at[k, j - 1],
            device_id={"tp": partner},
            device_id_type=MESH,
        )

    def fn_copy(xx):
        return pltpu.make_async_remote_copy(
            src_ref=arrived.at[xx * 2 + core, pl.ds(cap, cap)],
            dst_ref=arrived.at[xx * 2 + core, pl.ds(cap, cap)],
            send_sem=fn_send.at[xx],
            recv_sem=fn_recv.at[xx],
            device_id={"tp": partner},
            device_id_type=MESH,
        )

    def over_group(g, do, first=2):
        def one(k, _):
            @pl.when(k >= first)
            def _():
                do(k)

            return 0

        lax.fori_loop(g * group, (g + 1) * group, one, 0)

    def forward_first(g):
        def one(k):
            a2a_copy(k).wait_recv()
            for j in range(1, chips):
                fx_copy(k, j).start()
            fp_copy(k).start()

        over_group(g, one)

    def forward_second(g):
        def one(k):
            for j in range(1, chips):
                fx_copy(k, j).wait_recv()
                fq_copy(k, j).start()

        over_group(g, one)

    def forward_near():
        for xx in range(chips):
            near_copy(xx).wait_recv()
            fn_copy(xx).start()

    halo_copy.wait_recv()
    padded[pl.ds(0, halo), :] = jnp.where(me == 0, 0.0, halo_in[...].astype(f32))
    step_rows = 64
    window = step_rows + halo

    for lane in range(0, chan, 128):

        def conv_step(i, _):
            base = pl.multiple_of(i * step_rows, step_rows)
            rows_in = padded[pl.ds(base, window), lane : lane + 128]
            result = jnp.zeros((step_rows, 128), f32)
            for shift in range(8):
                turned = rows_in if shift == 0 else pltpu.roll(rows_in, window - shift, 0)
                for tap in range(reach):
                    offset = halo - tap
                    if offset % 8 == shift:
                        begin = offset - shift
                        result = (
                            result
                            + taps_ref[tap : tap + 1, lane : lane + 128]
                            * turned[begin : begin + step_rows]
                        )
            conv[pl.ds(base, step_rows), lane : lane + 128] = result
            return 0

        lax.fori_loop(0, length // step_rows, conv_step, 0)

    convolved = conv[...]
    sums = jnp.sum(convolved, axis=1, keepdims=True)
    squares = jnp.sum(convolved * convolved, axis=1, keepdims=True)
    lanes = lax.broadcasted_iota(jnp.int32, (length, 128), 1)
    packed = jnp.where(lanes == 0, sums, jnp.where(lanes == 1, squares, 0.0))
    stat_out[...] = jnp.transpose(packed)[0:8]

    def stat_copy(j):
        return pltpu.make_async_remote_copy(
            src_ref=stat_out,
            dst_ref=stat_in.at[j - 1],
            send_sem=stat_send.at[j - 1],
            recv_sem=stat_recv.at[j - 1],
            device_id={"tp": lax.rem(mine + j, tp)},
            device_id_type=MESH,
        )

    for j in range(1, tp):
        stat_copy(j).start()

    forward_near()
    forward_first(0)
    if groups > 1:
        forward_first(1)
    forward_second(0)

    stats = stat_out[...]
    for j in range(1, tp):
        stat_copy(j).wait_recv()
        stats = stats + stat_in[j - 1]
    stats = jnp.concatenate([stats, jnp.zeros((120, length), f32)], axis=0)
    columns = jnp.transpose(stats)
    mean = columns[:, 0:1] / (chan * tp)
    variance = columns[:, 1:2] / (chan * tp) - mean * mean
    scaled = (conv[...] - mean) * lax.rsqrt(variance + eps_norm) * ln_gain_ref[...]
    act[...] = jax.nn.silu(scaled).astype(bf16)

    def mix_copy(xx):
        return pltpu.make_async_remote_copy(
            src_ref=mix_out.at[xx],
            dst_ref=mix_in.at[xx],
            send_sem=mix_send.at[xx],
            recv_sem=mix_recv.at[xx],
            device_id={"tp": partner},
            device_id_type=MESH,
        )

    def mix_part(owner):
        begin = pl.multiple_of(owner * own_rows, own_rows)
        return jnp.dot(act[pl.ds(begin, own_rows), :], w_out[...], preferred_element_type=f32)

    loads[2].wait()

    def mix_first(xx, _):
        mix_out[xx] = mix_part(xx * 2 + 1 - core).astype(bf16)
        mix_copy(xx).start()
        return 0

    def mix_second(xx, _):
        mix_own[xx] = mix_part(xx * 2 + core).astype(bf16)
        return 0

    lax.fori_loop(0, chips, mix_first, 0)
    lax.fori_loop(0, chips, mix_second, 0)

    half = own_rows // 2

    def mix_x_copy(j, part):
        to, _ = across(j)
        span = pl.ds(part * half, half)
        return pltpu.make_async_remote_copy(
            src_ref=mix_x_out.at[j - 1, span],
            dst_ref=mix_x_in.at[j - 1, span],
            send_sem=mix_x_send.at[j - 1, part],
            recv_sem=mix_x_recv.at[j - 1, part],
            device_id={"tp": to},
            device_id_type=MESH,
        )

    def mix_stage():
        for xx in range(chips):
            mix_copy(xx).wait_recv()
        for j in range(1, chips):
            there = lax.rem(chip + j, chips)
            mix_x_out[j - 1] = (mix_own[there].astype(f32) + mix_in[there].astype(f32)).astype(
                bf16
            )
    loads[3].wait()
    loads[4].wait()
    loads[5].wait()

    def rs_copy(g, xx):
        return pltpu.make_async_remote_copy(
            src_ref=rs_out.at[g, xx],
            dst_ref=rs_in.at[g, xx],
            send_sem=rs_send.at[g, xx],
            recv_sem=rs_recv.at[g, xx],
            device_id={"tp": partner},
            device_id_type=MESH,
        )

    def rx_copy(k, j):
        to, _ = across(j)
        return pltpu.make_async_remote_copy(
            src_ref=rx_out.at[j - 1, block(k)],
            dst_ref=rx_in.at[j - 1, block(k)],
            send_sem=rx_send.at[k, j - 1],
            recv_sem=rx_recv.at[k, j - 1],
            device_id={"tp": to},
            device_id_type=MESH,
        )

    def ret_copy(k):
        return pltpu.make_async_remote_copy(
            src_ref=answer.at[block(k)],
            dst_ref=returned.at[block(k)],
            send_sem=ret_send.at[k],
            recv_sem=ret_recv.at[k],
            device_id={"ep": source(k)},
            device_id_type=MESH,
        )

    def expert_step(g):
        @pl.when(g == 0)
        def _():
            for xx in range(chips):
                fn_copy(xx).wait_recv()

        def one(k):
            fp_copy(k).wait_recv()
            for j in range(1, chips):
                fq_copy(k, j).wait_recv()

        over_group(g, one)
        span = pl.ds(pl.multiple_of(g * rows, rows), rows)
        x = jnp.concatenate([arrived[part, span] for part in range(tp)], axis=1)
        gate_act = jnp.dot(x, w_gate[...], preferred_element_type=f32)
        up_act = jnp.dot(x, w_up[...], preferred_element_type=f32)
        hidden = (jax.nn.silu(gate_act) * up_act).astype(bf16)
        for xx in range(chips):
            begin = pl.multiple_of((xx * 2 + 1 - core) * quarter, 128)
            rs_out[g, xx] = jnp.dot(
                hidden, w_down[:, pl.ds(begin, quarter)], preferred_element_type=f32
            ).astype(bf16)
            rs_copy(g, xx).start()
        for xx in range(chips):
            begin = pl.multiple_of((xx * 2 + core) * quarter, 128)
            rs_own[g, xx] = jnp.dot(
                hidden, w_down[:, pl.ds(begin, quarter)], preferred_element_type=f32
            ).astype(bf16)

    def sum_step(g):
        for xx in range(chips):
            rs_copy(g, xx).wait_recv()
        span = pl.ds(pl.multiple_of(g * rows, rows), rows)
        for j in range(1, chips):
            there = lax.rem(chip + j, chips)
            rx_out[j - 1, span] = (
                rs_own[g, there].astype(f32) + rs_in[g, there].astype(f32)
            ).astype(bf16)

        def one(k):
            for j in range(1, chips):
                rx_copy(k, j).start()

        over_group(g, one, 0)

    def return_step(g):
        def one(k):
            inner = pl.ds(pl.multiple_of((k - g * group) * cap, cap), cap)
            result = rs_own[g, chip, inner].astype(f32) + rs_in[g, chip, inner].astype(f32)
            for j in range(1, chips):
                rx_copy(k, j).wait_recv()
                result = result + rx_in[j - 1, block(k)].astype(f32)
            answer[block(k), :] = result.astype(bf16)

            @pl.when(k > 0)
            def _():
                ret_copy(k).start()

        over_group(g, one, 0)

    total[...] = jnp.zeros_like(total)

    def combine_step(g):
        def take(k, _):
            @pl.when(k > 0)
            def _():
                ret_copy(k).wait_recv()

            expert = toward(k)
            weight = jnp.where(ids_ref[:, 0:1] == expert, route_ref[:, 0:1], 0.0) + jnp.where(
                ids_ref[:, 1:2] == expert, route_ref[:, 1:2], 0.0
            )
            answers = returned[block(k), :]
            total[...] += weight * jnp.dot(onehots[k], answers, preferred_element_type=f32)
            return 0

        lax.fori_loop(g * group, (g + 1) * group, take, 0)

    def place_of(k, _):
        expert = toward(k)
        member = jnp.maximum(
            (ids_ref[:, 0:1] == expert).astype(f32), (ids_ref[:, 1:2] == expert).astype(f32)
        )
        member = jnp.broadcast_to(member, (tokens, cap))
        place = jnp.dot(below, member.astype(bf16), preferred_element_type=f32)
        slot = lax.broadcasted_iota(jnp.int32, (tokens, cap), 1).astype(f32)
        onehots[k] = jnp.where(place == slot, member, 0.0).astype(bf16)
        return 0

    def step(g, _):
        @pl.when(g < groups)
        def _():
            expert_step(g)

        @pl.when(g < groups)
        def _():
            sum_step(g)

        @pl.when(g + 1 < groups)
        def _():
            forward_second(g + 1)

        @pl.when(g == groups)
        def _():
            lax.fori_loop(0, n, place_of, 0)

        @pl.when((g >= 1) & (g < groups + 1))
        def _():
            return_step(g - 1)

        @pl.when(g == 0)
        def _():
            mix_stage()

        @pl.when(g + 2 < groups)
        def _():
            forward_first(g + 2)

        @pl.when(g == groups - 1)
        def _():
            for j in range(1, chips):
                mix_x_copy(j, 0).start()
                mix_x_copy(j, 1).start()

        return 0

    lax.fori_loop(0, groups + 1, step, 0)
    returned[0:cap, :] = answer[0:cap, :]

    def combine(g, _):
        combine_step(g)
        return 0

    lax.fori_loop(0, groups, combine, 0)
    expert_ref[...] = total[...].astype(bf16)

    mixed = mix_own[chip].astype(f32) + mix_in[chip].astype(f32)
    for j in range(1, chips):
        mix_x_copy(j, 0).wait_recv()
        mix_x_copy(j, 1).wait_recv()
        mixed = mixed + mix_x_in[j - 1].astype(f32)
    mixer_ref[...] = mixed.astype(bf16)

    ret_copy(1).wait_send()

    def left(k, _):
        a2a_copy(k).wait_send()
        ret_copy(k).wait_send()
        fp_copy(k).wait_send()
        for j in range(1, chips):
            fx_copy(k, j).wait_send()
            fq_copy(k, j).wait_send()
        return 0

    lax.fori_loop(2, n, left, 0)

    def left_x(k, _):
        for j in range(1, chips):
            rx_copy(k, j).wait_send()
        return 0

    lax.fori_loop(0, n, left_x, 0)
    halo_copy.wait_send()
    for j in range(1, tp):
        stat_copy(j).wait_send()
    for xx in range(chips):
        mix_copy(xx).wait_send()
        near_copy(xx).wait_send()
        fn_copy(xx).wait_send()
    for j in range(1, chips):
        mix_x_copy(j, 0).wait_send()
        mix_x_copy(j, 1).wait_send()

    def left_group(g, _):
        for xx in range(chips):
            rs_copy(g, xx).wait_send()
        return 0

    lax.fori_loop(0, groups, left_group, 0)


def on_device(
    glu_value,
    glu_gate,
    conv_kernel,
    ln_gain,
    out_weight,
    moe_input,
    moe_gain,
    gate_weight,
    up_weight,
    down_weight,
    expert_ids,
    route_weight,
):
    n = lax.axis_size("ep")
    tp = lax.axis_size("tp")
    chips = tp // 2
    length, chan = glu_value.shape
    reach = conv_kernel.shape[0]
    halo = -(-(reach - 1) // 16) * 16
    tokens, width = moe_input.shape
    hidden = gate_weight.shape[2]
    cap = 4 * max(1, tokens // n)
    group = max(1, min(n, 256 // cap))
    groups = n // group
    rows = group * cap
    quarter = width // tp
    own_rows = length // tp
    vmem = pl.BlockSpec(memory_space=pltpu.VMEM)
    hbm = pl.BlockSpec(memory_space=pl.ANY)
    dma = pltpu.SemaphoreType.DMA
    V = pltpu.VMEM
    others = max(1, chips - 1)
    return pl.pallas_call(
        functools.partial(kernel, n, tp, cap, group, reach),
        out_shape=(
            jax.ShapeDtypeStruct((own_rows, out_weight.shape[1]), bf16),
            jax.ShapeDtypeStruct((tokens, quarter), bf16),
        ),
        in_specs=[vmem] * 7 + [hbm] * 6,
        out_specs=(vmem, vmem),
        scratch_shapes=[
            V((length, chan), bf16),
            V((length, chan), bf16),
            V(out_weight.shape, bf16),
            V((width, hidden), bf16),
            V((width, hidden), bf16),
            V((hidden, width), bf16),
            dma((6,)),
            V((tokens, width), bf16),
            V((n * cap, quarter), bf16),
            V((chips, cap, quarter), bf16),
            V((n, tokens, cap), bf16),
            V((tp, n * cap, quarter), bf16),
            dma((chips,)),
            dma((chips,)),
            dma((chips,)),
            dma((chips,)),
            dma((n,)),
            dma((n,)),
            dma((n, others)),
            dma((n, others)),
            dma((n,)),
            dma((n,)),
            dma((n, others)),
            dma((n, others)),
            V((length, chan), bf16),
            V((halo, chan), bf16),
            dma,
            dma,
            V((length + halo, chan), f32),
            V((length, chan), f32),
            V((8, length), f32),
            V((tp - 1, 8, length), f32),
            dma((tp - 1,)),
            dma((tp - 1,)),
            V((length, chan), bf16),
            V((chips, own_rows, out_weight.shape[1]), bf16),
            V((chips, own_rows, out_weight.shape[1]), bf16),
            V((chips, own_rows, out_weight.shape[1]), bf16),
            dma((chips,)),
            dma((chips,)),
            V((others, own_rows, out_weight.shape[1]), bf16),
            V((others, own_rows, out_weight.shape[1]), bf16),
            dma((others, 2)),
            dma((others, 2)),
            V((groups, chips, rows, quarter), bf16),
            V((groups, chips, rows, quarter), bf16),
            V((groups, chips, rows, quarter), bf16),
            dma((groups, chips)),
            dma((groups, chips)),
            V((others, n * cap, quarter), bf16),
            V((others, n * cap, quarter), bf16),
            dma((n, others)),
            dma((n, others)),
            V((n * cap, quarter), bf16),
            V((n * cap, quarter), bf16),
            dma((n,)),
            dma((n,)),
            V((tokens, quarter), f32),
        ],
        compiler_params=pltpu.CompilerParams(
            collective_id=0, has_side_effects=True, vmem_limit_bytes=60 * 1024 * 1024
        ),
        name="block",
    )(
        moe_input,
        moe_gain.reshape(1, -1),
        expert_ids,
        expert_ids.T,
        route_weight,
        conv_kernel,
        ln_gain.reshape(1, -1),
        glu_value,
        glu_gate,
        out_weight,
        gate_weight,
        up_weight,
        down_weight,
    )


def solution(mesh):
    in_specs = (
        P("ep", "tp"),
        P("ep", "tp"),
        P(None, "tp"),
        P("tp"),
        P("tp", None),
        P("ep", None),
        P(),
        P("ep", None, "tp"),
        P("ep", None, "tp"),
        P("ep", "tp", None),
        P("ep", None),
        P("ep", None),
    )
    out_specs = (P(("ep", "tp"), None), P("ep", "tp"))
    return jax.shard_map(
        on_device, mesh=mesh, in_specs=in_specs, out_specs=out_specs, check_vma=False
    )
```

profile of v0, /device:TPU:16, one launch (start us, length us, event | category | flops | bytes accessed | tf_op | source)
XLA Modules:
  0.0 97.3 jit_solution(7988686204918951980)
XLA Ops:
  0.6 1.5 %copy.15.route_ref = f32[256,2]{1,0:T(8,128)} copy(f32[256,2]{0,1:T(2,128)} %param.23) | data formatting | bytes 4096 | tf_op args[11]
  2.1 1.5 %copy.14.ids_ref = s32[256,2]{1,0:T(8,128)} copy(s32[256,2]{0,1:T(2,128)} %param.22) | data formatting | bytes 4096 | tf_op args[10]
  3.6 90.1 %block.1 = (bf16[128,2048]{1,0:T(8,128)(2,1)}, bf16[256,512]{1,0:T(8,128)(2,1)}) custom-call(bf16[256,2048]{1,0:T(8,128)(2,1)} %moe_ref.1, f32[1,2048]{1,0:T(1,128)} %bitcast.3, s32[256,2]{1,0:T(8,128)} %copy.14.ids_ref, s32[2,256]{1,0:T(2,128)} %bitcast.4, f32[256,2]{1,0:T(8,128)} %copy.15.route_ref, f32[31,256]{1,0:T(8,128)} %taps_ref.1, ...), custom_call_target="tpu_custom_call" | custom-call | tf_op jit(solution)/shard_map/block/pallas_call | solution.py:670
  93.7 1.9 %copy.18 = bf16[128,2048]{1,0:T(8,128)(2,1)} copy(bf16[128,2048]{1,0:T(8,128)(2,1)} %get-tuple-element.4) | data formatting | bytes 1048576
  95.6 1.7 %copy.19 = bf16[256,512]{1,0:T(8,128)(2,1)} copy(bf16[256,512]{1,0:T(8,128)(2,1)} %get-tuple-element.5) | data formatting | bytes 524288
where the time goes:
time: 97.5 us; the launch traced here: 97.3 us
  Pallas kernels  90.1 us (92%)
  local copies, waits for them, and re-layouts  6.5 us (7%)
    pallas_call x1, Pallas kernels, on_device(): pl.pallas_call(functools.partial(kernel, n, tp, cap, group, reach), out_s...  90.1 us
    unnamed x4, local copies, waits for them, and re-layouts  6.5 us

commit v1 on v0

--- a/solution.py
+++ b/solution.py
@@ -20,13 +20,12 @@
     cap,
     group,
     reach,
-    moe_ref,
-    moe_gain_ref,
-    ids_ref,
-    ids_t_ref,
-    route_ref,
-    taps_ref,
-    ln_gain_ref,
+    moe_hbm,
+    moe_gain_hbm,
+    ids_t_hbm,
+    route_t_hbm,
+    taps_hbm,
+    ln_gain_hbm,
     value_hbm,
     gate_hbm,
     w_out_hbm,
@@ -93,6 +92,14 @@
     ret_send,
     ret_recv,
     total,
+    meta_ref,
+    moe_ref,
+    moe_gain_ref,
+    ids_t_ref,
+    route_t_ref,
+    taps_ref,
+    ln_gain_ref,
+    small_sem,
 ):
     me = lax.axis_index("ep")
     mine = lax.axis_index("tp")
@@ -152,12 +159,34 @@
             ]
         )
     ]
+    smalls = [
+        pltpu.make_async_copy(src, dst, small_sem.at[i])
+        for i, (src, dst) in enumerate(
+            [
+                (moe_hbm, moe_ref),
+                (moe_gain_hbm, moe_gain_ref),
+                (ids_t_hbm, ids_t_ref),
+                (route_t_hbm, route_t_ref),
+                (taps_hbm, taps_ref),
+                (ln_gain_hbm, ln_gain_ref),
+            ]
+        )
+    ]
+    for load in smalls:
+        load.start()
     for load in loads:
         load.start()
-
+    for load in smalls:
+        load.wait()
     everything = moe_ref[...].astype(f32)
     inverse = lax.rsqrt(jnp.sum(everything * everything, axis=1, keepdims=True) / width + eps_rms)
     normed[...] = (everything * inverse * moe_gain_ref[...]).astype(bf16)
+    lead = lax.broadcasted_iota(jnp.int32, (128, tokens), 0)
+    meta = jnp.where(lead == 0, ids_t_ref[0:1, :].astype(f32), 0.0)
+    meta = jnp.where(lead == 1, ids_t_ref[1:2, :].astype(f32), meta)
+    meta = jnp.where(lead == 2, route_t_ref[0:1, :], meta)
+    meta = jnp.where(lead == 3, route_t_ref[1:2, :], meta)
+    meta_ref[...] = jnp.transpose(meta)
     row = lax.broadcasted_iota(jnp.int32, (tokens, tokens), 0)
     col = lax.broadcasted_iota(jnp.int32, (tokens, tokens), 1)
     below = (col < row).astype(f32).astype(bf16)
@@ -204,12 +233,6 @@
         slots[block(k), :] = picked(slot_picks(k), mine)
         a2a_copy(k).start()
         return 0
-
-    lax.fori_loop(2, n, dispatch, 0)
-    pick = slot_picks(1)
-    for xx in range(chips):
-        near_slots[xx] = picked(pick, xx * 2 + core)
-        near_copy(xx).start()
 
     loads[0].wait()
     loads[1].wait()
@@ -225,6 +248,12 @@
     )
     halo_copy.start()
     padded[pl.ds(halo, length), :] = gated_now.astype(f32)
+
+    lax.fori_loop(2, n, dispatch, 0)
+    pick = slot_picks(1)
+    for xx in range(chips):
+        near_slots[xx] = picked(pick, xx * 2 + core)
+        near_copy(xx).start()
 
     pick = slot_picks(0)
     for part in range(tp):
@@ -522,8 +551,8 @@
                 ret_copy(k).wait_recv()
 
             expert = toward(k)
-            weight = jnp.where(ids_ref[:, 0:1] == expert, route_ref[:, 0:1], 0.0) + jnp.where(
-                ids_ref[:, 1:2] == expert, route_ref[:, 1:2], 0.0
+            weight = jnp.where(meta_ref[:, 0:1] == expert.astype(f32), meta_ref[:, 2:3], 0.0) + jnp.where(
+                meta_ref[:, 1:2] == expert.astype(f32), meta_ref[:, 3:4], 0.0
             )
             answers = returned[block(k), :]
             total[...] += weight * jnp.dot(onehots[k], answers, preferred_element_type=f32)
@@ -534,7 +563,7 @@
     def place_of(k, _):
         expert = toward(k)
         member = jnp.maximum(
-            (ids_ref[:, 0:1] == expert).astype(f32), (ids_ref[:, 1:2] == expert).astype(f32)
+            (meta_ref[:, 0:1] == expert.astype(f32)).astype(f32), (meta_ref[:, 1:2] == expert.astype(f32)).astype(f32)
         )
         member = jnp.broadcast_to(member, (tokens, cap))
         place = jnp.dot(below, member.astype(bf16), preferred_element_type=f32)
@@ -663,17 +692,17 @@
     quarter = width // tp
     own_rows = length // tp
     vmem = pl.BlockSpec(memory_space=pltpu.VMEM)
-    hbm = pl.BlockSpec(memory_space=pl.ANY)
+    hbm = pl.BlockSpec(memory_space=pltpu.HBM)
     dma = pltpu.SemaphoreType.DMA
     V = pltpu.VMEM
     others = max(1, chips - 1)
-    return pl.pallas_call(
+    mixed, routed = pl.pallas_call(
         functools.partial(kernel, n, tp, cap, group, reach),
         out_shape=(
-            jax.ShapeDtypeStruct((own_rows, out_weight.shape[1]), bf16),
-            jax.ShapeDtypeStruct((tokens, quarter), bf16),
+            pltpu.VMEM((own_rows, out_weight.shape[1]), bf16),
+            pltpu.VMEM((tokens, quarter), bf16),
         ),
-        in_specs=[vmem] * 7 + [hbm] * 6,
+        in_specs=[hbm] * 12,
         out_specs=(vmem, vmem),
         scratch_shapes=[
             V((length, chan), bf16),
@@ -734,17 +763,24 @@
             dma((n,)),
             dma((n,)),
             V((tokens, quarter), f32),
+            V((tokens, 128), f32),
+            V((tokens, width), bf16),
+            V((1, width), f32),
+            V(expert_ids.T.shape, jnp.int32),
+            V(route_weight.T.shape, f32),
+            V(conv_kernel.shape, f32),
+            V((1, chan), f32),
+            dma((6,)),
         ],
         compiler_params=pltpu.CompilerParams(
-            collective_id=0, has_side_effects=True, vmem_limit_bytes=60 * 1024 * 1024
+            collective_id=0, has_side_effects=True, vmem_limit_bytes=66_000_000
         ),
         name="block",
     )(
         moe_input,
         moe_gain.reshape(1, -1),
-        expert_ids,
         expert_ids.T,
-        route_weight,
+        route_weight.T,
         conv_kernel,
         ln_gain.reshape(1, -1),
         glu_value,
@@ -754,6 +790,32 @@
         up_weight,
         down_weight,
     )
+    return settle(
+        pltpu.with_memory_space_constraint(mixed, pltpu.VMEM),
+        pltpu.with_memory_space_constraint(routed, pltpu.VMEM),
+    )
+
+
+def settle_kernel(a_ref, b_ref, c_ref, d_ref, sem):
+    first = pltpu.make_async_copy(a_ref, c_ref, sem.at[0])
+    second = pltpu.make_async_copy(b_ref, d_ref, sem.at[1])
+    first.start()
+    second.start()
+    first.wait()
+    second.wait()
+
+
+def settle(a, b):
+    vmem = pl.BlockSpec(memory_space=pltpu.VMEM)
+    hbm = pl.BlockSpec(memory_space=pltpu.HBM)
+    return pl.pallas_call(
+        settle_kernel,
+        out_shape=(jax.ShapeDtypeStruct(a.shape, a.dtype), jax.ShapeDtypeStruct(b.shape, b.dtype)),
+        in_specs=[vmem, vmem],
+        out_specs=(hbm, hbm),
+        scratch_shapes=[pltpu.SemaphoreType.DMA((2,))],
+        name="settle",
+    )(a, b)
 
 
 def solution(mesh):

time: 97.5 us -> 85.9 us (0.88)
  the two profiles are of different devices: /device:TPU:16 before, /device:TPU:0 now
where the time goes in v1:
time: 85.9 us; the launch traced here: 85.8 us
  Pallas kernels  85.1 us (99%)
    pallas_call x1, Pallas kernels, on_device(): pl.pallas_call(functools.partial(kernel, n, tp, cap, group, reach), out_s...  84.2 us

profile of v1, /device:TPU:0, one launch (start us, length us, event | category | flops | bytes accessed | tf_op | source)
XLA Modules:
  0.0 85.8 jit_solution(10877006533734771168)
XLA Ops:
  0.6 84.2 %block.1 = (bf16[128,2048]{1,0:T(8,128)(2,1)S(1)}, bf16[256,512]{1,0:T(8,128)(2,1)S(1)}) custom-call(bf16[256,2048]{1,0:T(8,128)(2,1)} %moe_hbm.1, f32[1,2048]{1,0:T(1,128)} %bitcast.4, s32[2,256]{1,0:T(2,128)} %bitcast.5, f32[2,256]{1,0:T(2,128)} %bitcast.6, f32[31,256]{1,0:T(8,128)} %taps_hbm.1, f32[1,256]{1,0:T(1,128)} %bitcast.7, ...), custom_call_target="tpu_custom_call" | custom-call | tf_op jit(solution)/shard_map/block/pallas_call | solution.py:699
  84.9 0.9 %settle.1 = (bf16[128,2048]{1,0:T(8,128)(2,1)}, bf16[256,512]{1,0:T(8,128)(2,1)}) custom-call(bf16[128,2048]{1,0:T(8,128)(2,1)S(1)} %get-tuple-element.4.a_ref, bf16[256,512]{1,0:T(8,128)(2,1)S(1)} %get-tuple-element.5.b_ref), custom_call_target="tpu_custom_call" | custom-call | tf_op jit(solution)/shard_map/settle/pallas_call | solution.py:811

commit v2 on v1

--- a/solution.py
+++ b/solution.py
@@ -1,4 +1,5 @@
 import functools
+import types
 
 import jax
 import jax.numpy as jnp
@@ -663,6 +664,803 @@
     lax.fori_loop(0, groups, left_group, 0)
 
 
+def line_kernel(n, tp, cap, reach, near, names, *refs):
+    r = types.SimpleNamespace(**dict(zip(names, refs)))
+    me = lax.axis_index("ep")
+    mine = lax.axis_index("tp")
+    core = lax.rem(mine, 2)
+    chip = mine // 2
+    partner = chip * 2 + 1 - core
+    across = (1 - chip) * 2 + core
+    stations = n // 2
+    z = me // 2
+    y = lax.rem(me, 2)
+    beside = z * 2 + 1 - y
+    tokens, width = r.moe.shape
+    quarter = width // tp
+    length, chan = r.value.shape
+    halo = r.halo_in.shape[0]
+    own_rows = length // tp
+    behind = jnp.minimum(z, stations - 1 - z)
+    inner = behind >= 1
+    longer = jnp.where(stations - 1 - z > z, 1, -1)
+
+    def distance(j):
+        return jnp.where(j <= 2 * behind, (j + 1) // 2, j - behind)
+
+    def origin(j):
+        turn = jnp.where((j <= 2 * behind) & (lax.rem(j, 2) == 1), -longer, longer)
+        return z + turn * distance(j)
+
+    def home(s):
+        return origin(s // 2) * 2 + lax.rem(y + s, 2)
+
+    def block(k):
+        return pl.ds(pl.multiple_of(k * cap, cap), cap)
+
+    def remote(src, dst, send, recv, **device):
+        return pltpu.make_async_remote_copy(
+            src_ref=src,
+            dst_ref=dst,
+            send_sem=send,
+            recv_sem=recv,
+            device_id=device,
+            device_id_type=MESH,
+        )
+
+    barrier = pltpu.get_barrier_semaphore()
+
+    def greet_ep(k, _):
+        pl.semaphore_signal(
+            barrier, inc=1, device_id={"ep": lax.rem(me + k, n)}, device_id_type=MESH
+        )
+        return 0
+
+    lax.fori_loop(1, n, greet_ep, 0)
+    for j in range(1, tp):
+        pl.semaphore_signal(
+            barrier, inc=1, device_id={"tp": lax.rem(mine + j, tp)}, device_id_type=MESH
+        )
+
+    loads = {
+        name: pltpu.make_async_copy(src, dst, r.load_sem.at[i])
+        for i, (name, src, dst) in enumerate(
+            [
+                ("moe", r.moe_hbm, r.moe),
+                ("moe_gain", r.moe_gain_hbm, r.moe_gain),
+                ("ids", r.ids_hbm, r.ids),
+                ("route", r.route_hbm, r.route),
+                ("value", r.value_hbm, r.value),
+                ("gate", r.gate_hbm, r.gate),
+                ("taps", r.taps_hbm, r.taps),
+                ("ln_gain", r.ln_gain_hbm, r.ln_gain),
+                ("w_gate", r.w_gate_hbm.at[0], r.w_gate),
+                ("w_up", r.w_up_hbm.at[0], r.w_up),
+                ("w_down", r.w_down_hbm.at[0], r.w_down),
+                ("w_out", r.w_out_hbm, r.w_out),
+            ]
+        )
+    }
+    late = ("w_gate", "w_up", "w_down", "w_out")
+    for name, load in loads.items():
+        if name not in late:
+            load.start()
+
+    def own_copy(up, xx):
+        return remote(
+            r.normed.at[xx * 2 + core],
+            r.tok.at[z, xx],
+            r.own_send.at[up, xx],
+            r.tok_recv.at[z, xx],
+            ep=(z + 2 * up - 1) * 2 + y,
+        )
+
+    def own_ids(up):
+        return remote(
+            r.ids_all.at[z],
+            r.ids_all.at[z],
+            r.ids_own_send.at[up],
+            r.ids_recv.at[z],
+            ep=(z + 2 * up - 1) * 2 + y,
+        )
+
+    def onward(zz):
+        return jnp.where(zz < z, z + 1, z - 1)
+
+    def pass_copy(zz, xx):
+        return remote(
+            r.tok.at[zz, xx],
+            r.tok.at[zz, xx],
+            r.pass_send.at[zz, xx],
+            r.tok_recv.at[zz, xx],
+            ep=onward(zz) * 2 + y,
+        )
+
+    def pass_ids(zz):
+        return remote(
+            r.ids_all.at[zz],
+            r.ids_all.at[zz],
+            r.ids_pass_send.at[zz],
+            r.ids_recv.at[zz],
+            ep=onward(zz) * 2 + y,
+        )
+
+    def side_copy(j, xx):
+        return remote(
+            r.side.at[j, xx],
+            r.arrived.at[xx * 2 + core, block(2 * j + 1)],
+            r.side_send.at[j, xx],
+            r.side_recv.at[j, xx],
+            ep=beside,
+        )
+
+    def slant_copy(j):
+        return remote(
+            r.side.at[j, chip],
+            r.arrived.at[mine, block(2 * j + 1)],
+            r.slant_send.at[j],
+            r.side_recv.at[j, chip],
+            ep=beside,
+            tp=across,
+        )
+
+    def core_copy(s, xx):
+        return remote(
+            r.arrived.at[xx * 2 + core, block(s)],
+            r.arrived.at[xx * 2 + core, block(s)],
+            r.core_send.at[s, xx],
+            r.core_recv.at[s, xx],
+            tp=partner,
+        )
+
+    def cross_copy(s):
+        return remote(
+            r.arrived.at[mine, block(s)],
+            r.arrived.at[mine, block(s)],
+            r.cross_send.at[s],
+            r.cross_recv.at[s],
+            tp=across,
+        )
+
+    def rs_copy(s, xx):
+        return remote(
+            r.rs_out.at[s, xx], r.rs_in.at[s, xx], r.rs_send.at[s, xx], r.rs_recv.at[s, xx], tp=partner
+        )
+
+    def rx_copy(s):
+        return remote(r.rx_out.at[s], r.rx_in.at[s], r.rx_send.at[s], r.rx_recv.at[s], tp=across)
+
+    def ret_copy(s):
+        return remote(
+            r.answer.at[s], r.returned.at[me], r.ret_send.at[s], r.ret_recv.at[me], ep=home(s)
+        )
+
+    def ret_arrival(s):
+        there = home(s)
+        return remote(
+            r.answer.at[s], r.returned.at[there], r.ret_send.at[s], r.ret_recv.at[there], ep=there
+        )
+
+    halo_copy = remote(
+        r.gated.at[pl.ds(length - halo, halo)],
+        r.halo_in,
+        r.halo_send,
+        r.halo_recv,
+        ep=lax.rem(me + 1, n),
+    )
+
+    def stat_copy(j):
+        return remote(
+            r.stat_out,
+            r.stat_in.at[j - 1],
+            r.stat_send.at[j - 1],
+            r.stat_recv.at[j - 1],
+            tp=lax.rem(mine + j, tp),
+        )
+
+    def mix_copy(xx):
+        return remote(r.mix_out.at[xx], r.mix_in.at[xx], r.mix_send.at[xx], r.mix_recv.at[xx], tp=partner)
+
+    pieces = r.mix_x_send.shape[0]
+    piece = own_rows // pieces
+
+    def mix_x_copy(part):
+        span = pl.ds(pl.multiple_of(part * piece, piece), piece)
+        return remote(
+            r.mix_x_out.at[span], r.mix_x_in.at[span], r.mix_x_send.at[part], r.mix_x_recv.at[part], tp=across
+        )
+
+    loads["moe"].wait()
+    loads["moe_gain"].wait()
+    everything = r.moe[...].astype(f32)
+    inverse = lax.rsqrt(jnp.sum(everything * everything, axis=1, keepdims=True) / width + eps_rms)
+    normed_now = (everything * inverse * r.moe_gain[...]).astype(bf16)
+    for part in range(tp):
+        r.normed[part] = normed_now[:, part * quarter : (part + 1) * quarter]
+    loads["ids"].wait()
+    loads["route"].wait()
+    r.ids_all[z] = jnp.concatenate([r.ids[...].astype(f32), jnp.zeros((6, tokens), f32)], axis=0)
+    for name in late:
+        loads[name].start()
+    loads["value"].wait()
+    loads["gate"].wait()
+    gated_now = (r.value[...].astype(f32) * jax.nn.sigmoid(r.gate[...].astype(f32))).astype(bf16)
+    r.gated[...] = gated_now
+    r.padded[pl.ds(halo, length), :] = gated_now.astype(f32)
+
+    pl.semaphore_wait(barrier, n - 1 + tp - 1)
+    halo_copy.start()
+
+    def each_way(do):
+        @pl.when(z > 0)
+        def _():
+            do(0)
+
+        @pl.when(z < stations - 1)
+        def _():
+            do(1)
+
+    each_way(lambda up: own_ids(up).start())
+    each_way(lambda up: own_copy(up, chip).start())
+    if near > 1:
+        each_way(lambda up: own_copy(up, 1 - chip).start())
+
+    row = lax.broadcasted_iota(jnp.int32, (tokens, tokens), 0)
+    col = lax.broadcasted_iota(jnp.int32, (tokens, tokens), 1)
+    r.above[...] = (row < col).astype(f32).astype(bf16)
+    slot_rows = lax.broadcasted_iota(jnp.int32, (cap, tokens), 0).astype(f32)
+
+    def choices(zz):
+        here = (z * 2 + lax.rem(y + lax.broadcasted_iota(jnp.int32, (16, tokens), 0), 2)).astype(f32)
+        chosen = r.ids_all[zz]
+        member = jnp.maximum(
+            (chosen[0:1, :] == here).astype(f32), (chosen[1:2, :] == here).astype(f32)
+        )
+        place = jnp.dot(member.astype(bf16), r.above[...], preferred_element_type=f32)
+        key = jnp.where(member > 0.0, place, -1.0)
+        ours = (slot_rows == key[0:1, :]).astype(f32).astype(bf16)
+        theirs = (slot_rows == key[1:2, :]).astype(f32).astype(bf16)
+        return ours, theirs
+
+    ours, theirs = choices(z)
+    for xx in (chip, 1 - chip):
+        r.side[0, xx] = jnp.dot(
+            theirs, r.normed[xx * 2 + core], preferred_element_type=f32
+        ).astype(bf16)
+        side_copy(0, xx).start()
+    for part in range(tp):
+        r.arrived[part, block(0), :] = jnp.dot(
+            ours, r.normed[part], preferred_element_type=f32
+        ).astype(bf16)
+
+    def expert_step(s, first=False):
+        def partial(part):
+            rows = pl.ds(pl.multiple_of(part * quarter, quarter), quarter)
+            x = r.arrived[part, block(s)]
+            return (
+                jnp.dot(x, r.w_gate[rows, :], preferred_element_type=f32),
+                jnp.dot(x, r.w_up[rows, :], preferred_element_type=f32),
+            )
+
+        gate_act, up_act = partial(core)
+        more = partial(2 + core)
+        gate_act, up_act = gate_act + more[0], up_act + more[1]
+        for xx in range(2):
+            if not first:
+                core_copy(s, xx).wait_recv()
+            more = partial(xx * 2 + 1 - core)
+            gate_act, up_act = gate_act + more[0], up_act + more[1]
+        hidden = (jax.nn.silu(gate_act) * up_act).astype(bf16)
+        for xx in (1 - chip, chip):
+            begin = pl.multiple_of((xx * 2 + 1 - core) * quarter, 128)
+            r.rs_out[s, xx] = jnp.dot(
+                hidden, r.w_down[:, pl.ds(begin, quarter)], preferred_element_type=f32
+            ).astype(bf16)
+            rs_copy(s, xx).start()
+        for xx in (1 - chip, chip):
+            begin = pl.multiple_of((xx * 2 + core) * quarter, 128)
+            r.rs_own[s, xx] = jnp.dot(
+                hidden, r.w_down[:, pl.ds(begin, quarter)], preferred_element_type=f32
+            ).astype(bf16)
+
+    def sum_step(s):
+        rs_copy(s, 1 - chip).wait_recv()
+        r.rx_out[s] = (r.rs_own[s, 1 - chip].astype(f32) + r.rs_in[s, 1 - chip].astype(f32)).astype(bf16)
+        rx_copy(s).start()
+
+    def return_step(s):
+        rs_copy(s, chip).wait_recv()
+        rx_copy(s).wait_recv()
+        result = r.rs_own[s, chip].astype(f32) + r.rs_in[s, chip].astype(f32)
+        r.answer[s] = (result + r.rx_in[s].astype(f32)).astype(bf16)
+
+        @pl.when(s > 0)
+        def _():
+            ret_copy(s).start()
+
+    loads["taps"].wait()
+    step_rows = 64
+    window = step_rows + halo
+
+    def conv_rows(lane, begin, end):
+        def conv_step(i, _):
+            base = pl.multiple_of(i * step_rows, step_rows)
+            rows_in = r.padded[pl.ds(base, window), lane : lane + 128]
+            result = jnp.zeros((step_rows, 128), f32)
+            for shift in range(8):
+                turned = rows_in if shift == 0 else pltpu.roll(rows_in, window - shift, 0)
+                for tap in range(reach):
+                    offset = halo - tap
+                    if offset % 8 == shift:
+                        begin = offset - shift
+                        result = (
+                            result
+                            + r.taps[tap : tap + 1, lane : lane + 128]
+                            * turned[begin : begin + step_rows]
+                        )
+            r.conv[pl.ds(base, step_rows), lane : lane + 128] = result
+            return 0
+
+        lax.fori_loop(begin, end, conv_step, 0)
+
+    for lane in range(0, chan, 128):
+        conv_rows(lane, 1, length // step_rows)
+    lead = lax.broadcasted_iota(jnp.int32, (128, tokens), 0)
+    meta = jnp.where(lead == 0, r.ids[0:1, :].astype(f32), 0.0)
+    meta = jnp.where(lead == 1, r.ids[1:2, :].astype(f32), meta)
+    meta = jnp.where(lead == 2, r.route[0:1, :], meta)
+    meta = jnp.where(lead == 3, r.route[1:2, :], meta)
+    meta = jnp.transpose(meta)
+    order = lax.broadcasted_iota(jnp.int32, (tokens, 128), 1)
+    expert = home(order).astype(f32)
+    first = (meta[:, 0:1] == expert) & (order < n)
+    second = (meta[:, 1:2] == expert) & (order < n)
+    member = jnp.maximum(first.astype(f32), second.astype(f32))
+    below = (col < row).astype(f32).astype(bf16)
+    place = jnp.dot(below, member.astype(bf16), preferred_element_type=f32)
+    key = jnp.where(member > 0.0, place, -1.0)
+    weights = jnp.where(first, meta[:, 2:3], 0.0) + jnp.where(second, meta[:, 3:4], 0.0)
+    r.key[...] = key
+    r.weights[...] = weights
+    halo_copy.wait_recv()
+    r.padded[pl.ds(0, halo), :] = jnp.where(me == 0, 0.0, r.halo_in[...].astype(f32))
+    for lane in range(0, chan, 128):
+        conv_rows(lane, 0, 1)
+
+    convolved = r.conv[...]
+    sums = jnp.sum(convolved, axis=1, keepdims=True)
+    squares = jnp.sum(convolved * convolved, axis=1, keepdims=True)
+    lanes = lax.broadcasted_iota(jnp.int32, (length, 128), 1)
+    packed = jnp.where(lanes == 0, sums, jnp.where(lanes == 1, squares, 0.0))
+    r.stat_out[...] = jnp.transpose(packed)[0:8]
+    for j in range(1, tp):
+        stat_copy(j).start()
+
+    loads["w_gate"].wait()
+    loads["w_up"].wait()
+    loads["w_down"].wait()
+    expert_step(0, first=True)
+
+    loads["ln_gain"].wait()
+    loads["w_out"].wait()
+    sum_step(0)
+    stats = r.stat_out[...]
+    for j in range(1, tp):
+        stat_copy(j).wait_recv()
+        stats = stats + r.stat_in[j - 1]
+    stats = jnp.concatenate([stats, jnp.zeros((120, length), f32)], axis=0)
+    columns = jnp.transpose(stats)
+    mean = columns[:, 0:1] / (chan * tp)
+    variance = columns[:, 1:2] / (chan * tp) - mean * mean
+    scaled = (r.conv[...] - mean) * lax.rsqrt(variance + eps_norm) * r.ln_gain[...]
+    r.act[...] = jax.nn.silu(scaled).astype(bf16)
+
+    def mix_part(owner):
+        begin = pl.multiple_of(owner * own_rows, own_rows)
+        return jnp.dot(r.act[pl.ds(begin, own_rows), :], r.w_out[...], preferred_element_type=f32)
+
+    for xx in (1 - chip, chip):
+        r.mix_out[xx] = mix_part(xx * 2 + 1 - core).astype(bf16)
+        mix_copy(xx).start()
+        r.mix_own[xx] = mix_part(xx * 2 + core).astype(bf16)
+    mix_copy(1 - chip).wait_recv()
+    for part in range(pieces):
+        span = pl.ds(part * piece, piece)
+        r.mix_x_out[span] = (
+            r.mix_own[1 - chip, span].astype(f32) + r.mix_in[1 - chip, span].astype(f32)
+        ).astype(bf16)
+    mix_x_copy(0).start()
+
+    def pull(j):
+        zz = origin(j)
+        there = onward(zz)
+        pass_ids(zz).wait_recv()
+        pass_copy(zz, chip).wait_recv()
+
+        @pl.when((there >= 0) & (there < stations))
+        def _():
+            pass_ids(zz).start()
+            pass_copy(zz, chip).start()
+
+    def pull_rest(j):
+        zz = origin(j)
+        there = onward(zz)
+        pass_copy(zz, 1 - chip).wait_recv()
+
+        @pl.when((there >= 0) & (there < stations) & (distance(j) + 1 < near))
+        def _():
+            pass_copy(zz, 1 - chip).start()
+
+    def absorb(j):
+        zz = origin(j)
+        full = distance(j) < near
+
+        @pl.when(full)
+        def _():
+            pull_rest(j)
+
+        ours, theirs = choices(zz)
+        both = jnp.concatenate([ours, theirs], axis=0)
+
+        def spread(xx):
+            rows = jnp.dot(both, r.tok[zz, xx], preferred_element_type=f32).astype(bf16)
+            r.side[j, xx] = rows[cap:]
+            r.arrived[xx * 2 + core, block(2 * j), :] = rows[:cap]
+            side_copy(j, xx).start()
+
+            @pl.when(jnp.logical_not(full))
+            def _():
+                cross_copy(2 * j).start()
+                slant_copy(j).start()
+
+            core_copy(2 * j, xx).start()
+
+        spread(chip)
+
+        @pl.when(full)
+        def _():
+            spread(1 - chip)
+
+    def gather_side(j):
+        for xx in (chip, 1 - chip):
+            side_copy(j, xx).wait_recv()
+            core_copy(2 * j + 1, xx).start()
+
+    def gather_cross(s):
+        @pl.when((distance(s // 2) >= near) & (lax.rem(s, 2) == 0))
+        def _():
+            cross_copy(s).wait_recv()
+            core_copy(s, 1 - chip).start()
+
+    @pl.when(inner)
+    def _():
+        pull(1)
+        pull(2)
+
+    plan = schedule(stations)
+    early = min(pieces - 1, 2)
+
+    def entry(name, i):
+        found = jnp.int32(-1)
+        for k, (end, mid) in enumerate(plan[name]):
+            found = jnp.where(i == k, jnp.where(inner, mid, end), found)
+        return found
+
+    def step(i, _):
+        a = entry("arrive", i)
+        e = entry("expert", i)
+        b = entry("answer", i)
+        c = entry("pull", i)
+        d = entry("sum", i)
+        j = a // 2
+
+        @pl.when(c >= 0)
+        def _():
+            pull(c)
+
+        @pl.when((a >= 0) & (lax.rem(a, 2) == 0))
+        def _():
+            @pl.when(jnp.logical_not(inner))
+            def _():
+                pull(j)
+
+            absorb(j)
+
+        @pl.when((a >= 0) & (lax.rem(a, 2) == 1))
+        def _():
+            gather_side(j)
+
+        @pl.when(e >= 0)
+        def _():
+            gather_cross(e)
+            expert_step(e)
+
+        @pl.when(b >= 0)
+        def _():
+            return_step(b)
+
+        @pl.when(d >= 0)
+        def _():
+            sum_step(d)
+
+        @pl.when((i + 1 <= early) & jnp.logical_not(inner))
+        def _():
+            mix_x_copy(i + 1).start()
+
+        return 0
+
+    lax.fori_loop(0, len(plan["arrive"]), step, 0)
+
+    slot_columns = lax.broadcasted_iota(jnp.int32, (tokens, cap), 1).astype(f32)
+
+    def take(s):
+        onehot = (r.key[:, s : s + 1] == slot_columns).astype(f32).astype(bf16)
+        if s > 0:
+            ret_arrival(s).wait_recv()
+            rows = r.returned[home(s)]
+        else:
+            rows = r.answer[0]
+        return r.weights[:, s : s + 1] * jnp.dot(onehot, rows, preferred_element_type=f32)
+
+    for part in range(1, pieces):
+        if part > early:
+            mix_x_copy(part).start()
+        else:
+
+            @pl.when(inner)
+            def _():
+                mix_x_copy(part).start()
+
+    for k in range(len(plan["finish"])):
+        b = jnp.where(inner, *reversed(plan["finish"][k]))
+
+        @pl.when(b >= 0)
+        def _():
+            return_step(b)
+
+        if k == 0:
+            r.total[...] = take(0)
+        elif k == 1:
+            r.total[...] += take(1)
+
+    mix_copy(chip).wait_recv()
+    mixed = r.mix_own[chip].astype(f32) + r.mix_in[chip].astype(f32)
+    for part in range(pieces):
+        mix_x_copy(part).wait_recv()
+    r.mixer_out[...] = (mixed + r.mix_x_in[...].astype(f32)).astype(bf16)
+    for s in range(2, n - 1):
+        r.total[...] += take(s)
+    r.expert_out[...] = (r.total[...] + take(n - 1)).astype(bf16)
+
+    each_way(lambda up: own_ids(up).wait_send())
+    each_way(lambda up: own_copy(up, chip).wait_send())
+    if near > 1:
+        each_way(lambda up: own_copy(up, 1 - chip).wait_send())
+
+    def left(j, _):
+        zz = origin(j)
+        there = onward(zz)
+        full = distance(j) < near
+
+        @pl.when((there >= 0) & (there < stations))
+        def _():
+            pass_ids(zz).wait_send()
+            pass_copy(zz, chip).wait_send()
+
+            @pl.when(distance(j) + 1 < near)
+            def _():
+                pass_copy(zz, 1 - chip).wait_send()
+
+        side_copy(j, chip).wait_send()
+
+        @pl.when(full)
+        def _():
+            side_copy(j, 1 - chip).wait_send()
+
+        for s in (2 * j, 2 * j + 1):
+            for xx in range(2):
+                core_copy(s, xx).wait_send()
+
+        @pl.when(jnp.logical_not(full))
+        def _():
+            cross_copy(2 * j).wait_send()
+            slant_copy(j).wait_send()
+
+        return 0
+
+    lax.fori_loop(1, stations, left, 0)
+    for xx in range(2):
+        side_copy(0, xx).wait_send()
+        core_copy(1, xx).wait_send()
+        mix_copy(xx).wait_send()
+
+    def left_more(s, _):
+        for xx in range(2):
+            rs_copy(s, xx).wait_send()
+        rx_copy(s).wait_send()
+
+        @pl.when(s > 0)
+        def _():
+            ret_copy(s).wait_send()
+
+        return 0
+
+    lax.fori_loop(0, n, left_more, 0)
+    halo_copy.wait_send()
+    for j in range(1, tp):
+        stat_copy(j).wait_send()
+    for part in range(pieces):
+        mix_x_copy(part).wait_send()
+
+
+def schedule(stations):
+    total = 2 * stations
+    if stations == 4:
+        ends = dict(
+            arrive=[1, 2, 3, 4, 6, 5, -1, 7],
+            expert=[1, 2, 3, 4, -1, 5, 6, 7],
+            sum=[1, 2, 3, -1, 4, 5, 6, 7],
+            answer=[-1, 0, 1, 2, -1, 3, -1, 4],
+            finish=[5, 6, 7],
+        )
+        mids = dict(
+            arrive=[1, 2, 4, 3, 6, 5, 7],
+            expert=[1, 2, 4, 3, 6, 5, 7],
+            answer=[-1, 0, -1, -1, 4, 1, 6],
+            sum=[1, 2, 4, 3, 6, 5, 7],
+            pull=[-1, -1, -1, 3],
+            finish=[2, 5, 3, 7],
+        )
+    else:
+        arrive = [1] + list(range(2, total, 2)) + list(range(3, total, 2))
+        ends = dict(arrive=arrive, expert=[1] + [-1] * (total - 2) + list(range(2, total)))
+        ends["finish"] = list(range(total))
+        ends["sum"] = ends["expert"]
+        mids = dict(ends, pull=[-1] + list(range(3, stations)))
+    plan = {}
+    steps = max(len(part) for part in list(ends.values()) + list(mids.values()))
+    for name in ("arrive", "expert", "sum", "answer", "pull", "finish"):
+        one, two = ends.get(name, []), mids.get(name, [])
+        used = max(len(one), len(two)) if name == "finish" else steps
+        plan[name] = [tuple((part + [-1] * used)[k] for part in (one, two)) for k in range(used)]
+    return plan
+
+
+def line_call(
+    near,
+    glu_value,
+    glu_gate,
+    conv_kernel,
+    ln_gain,
+    out_weight,
+    moe_input,
+    moe_gain,
+    gate_weight,
+    up_weight,
+    down_weight,
+    expert_ids,
+    route_weight,
+):
+    n = lax.axis_size("ep")
+    tp = lax.axis_size("tp")
+    stations = n // 2
+    length, chan = glu_value.shape
+    reach = conv_kernel.shape[0]
+    halo = -(-(reach - 1) // 16) * 16
+    tokens, width = moe_input.shape
+    hidden = gate_weight.shape[2]
+    cap = 4 * max(1, tokens // n)
+    quarter = width // tp
+    own_rows = length // tp
+    out_width = out_weight.shape[1]
+    top = expert_ids.shape[1]
+    dma = pltpu.SemaphoreType.DMA
+    V = pltpu.VMEM
+    pieces = 4
+    scratch = dict(
+        moe=V((tokens, width), bf16),
+        moe_gain=V((1, width), f32),
+        ids=V((top, tokens), jnp.int32),
+        route=V((top, tokens), f32),
+        value=V((length, chan), bf16),
+        gate=V((length, chan), bf16),
+        taps=V((reach, chan), f32),
+        ln_gain=V((1, chan), f32),
+        w_gate=V((width, hidden), bf16),
+        w_up=V((width, hidden), bf16),
+        w_down=V((hidden, width), bf16),
+        w_out=V((chan, out_width), bf16),
+        load_sem=dma((12,)),
+        normed=V((tp, tokens, quarter), bf16),
+        ids_all=V((stations, 8, tokens), f32),
+        above=V((tokens, tokens), bf16),
+        tok=V((stations, 2, tokens, quarter), bf16),
+        side=V((stations, 2, cap, quarter), bf16),
+        arrived=V((tp, n * cap, quarter), bf16),
+        own_send=dma((2, 2)),
+        tok_recv=dma((stations, 2)),
+        ids_own_send=dma((2,)),
+        ids_recv=dma((stations,)),
+        pass_send=dma((stations, 2)),
+        ids_pass_send=dma((stations,)),
+        side_send=dma((stations, 2)),
+        side_recv=dma((stations, 2)),
+        core_send=dma((n, 2)),
+        core_recv=dma((n, 2)),
+        cross_send=dma((n,)),
+        cross_recv=dma((n,)),
+        gated=V((length, chan), bf16),
+        halo_in=V((halo, chan), bf16),
+        halo_send=dma,
+        halo_recv=dma,
+        padded=V((length + halo, chan), f32),
+        conv=V((length, chan), f32),
+        stat_out=V((8, length), f32),
+        stat_in=V((tp - 1, 8, length), f32),
+        stat_send=dma((tp - 1,)),
+        stat_recv=dma((tp - 1,)),
+        act=V((length, chan), bf16),
+        mix_out=V((2, own_rows, out_width), bf16),
+        mix_own=V((2, own_rows, out_width), bf16),
+        mix_in=V((2, own_rows, out_width), bf16),
+        mix_send=dma((2,)),
+        mix_recv=dma((2,)),
+        mix_x_out=V((own_rows, out_width), bf16),
+        mix_x_in=V((own_rows, out_width), bf16),
+        mix_x_send=dma((pieces,)),
+        mix_x_recv=dma((pieces,)),
+        rs_out=V((n, 2, cap, quarter), bf16),
+        rs_own=V((n, 2, cap, quarter), bf16),
+        rs_in=V((n, 2, cap, quarter), bf16),
+        rs_send=dma((n, 2)),
+        rs_recv=dma((n, 2)),
+        rx_out=V((n, cap, quarter), bf16),
+        rx_in=V((n, cap, quarter), bf16),
+        rx_send=dma((n,)),
+        rx_recv=dma((n,)),
+        answer=V((n, cap, quarter), bf16),
+        returned=V((n, cap, quarter), bf16),
+        ret_send=dma((n,)),
+        ret_recv=dma((n,)),
+        total=V((tokens, quarter), f32),
+        key=V((tokens, 128), f32),
+        weights=V((tokens, 128), f32),
+        slant_send=dma((stations,)),
+    )
+    operands = dict(
+        moe_hbm=moe_input,
+        moe_gain_hbm=moe_gain.reshape(1, -1),
+        ids_hbm=expert_ids.T,
+        route_hbm=route_weight.T,
+        value_hbm=glu_value,
+        gate_hbm=glu_gate,
+        taps_hbm=conv_kernel,
+        ln_gain_hbm=ln_gain.reshape(1, -1),
+        w_gate_hbm=gate_weight,
+        w_up_hbm=up_weight,
+        w_down_hbm=down_weight,
+        w_out_hbm=out_weight,
+    )
+    names = tuple(operands) + ("mixer_out", "expert_out") + tuple(scratch)
+    hbm = pl.BlockSpec(memory_space=pltpu.HBM)
+    vmem = pl.BlockSpec(memory_space=pltpu.VMEM)
+    mixed, routed = pl.pallas_call(
+        functools.partial(line_kernel, n, tp, cap, reach, near, names),
+        out_shape=(V((own_rows, out_width), bf16), V((tokens, quarter), bf16)),
+        in_specs=[hbm] * len(operands),
+        out_specs=(vmem, vmem),
+        scratch_shapes=list(scratch.values()),
+        compiler_params=pltpu.CompilerParams(
+            collective_id=0, has_side_effects=True, vmem_limit_bytes=66_000_000
+        ),
+        name="line",
+    )(*operands.values())
+    return settle(
+        pltpu.with_memory_space_constraint(mixed, pltpu.VMEM),
+        pltpu.with_memory_space_constraint(routed, pltpu.VMEM),
+    )
+
+
 def on_device(
     glu_value,
     glu_gate,
@@ -680,6 +1478,22 @@
     n = lax.axis_size("ep")
     tp = lax.axis_size("tp")
     chips = tp // 2
+    if chips == 2 and (n // 2) * moe_input.shape[0] <= n * 4 * max(1, moe_input.shape[0] // n):
+        return line_call(
+            3,
+            glu_value,
+            glu_gate,
+            conv_kernel,
+            ln_gain,
+            out_weight,
+            moe_input,
+            moe_gain,
+            gate_weight,
+            up_weight,
+            down_weight,
+            expert_ids,
+            route_weight,
+        )
     length, chan = glu_value.shape
     reach = conv_kernel.shape[0]
     halo = -(-(reach - 1) // 16) * 16

time: 85.9 us -> 68.8 us (0.80)
  Pallas kernels: 85.1 us -> 68 us
    pallas_call x1, Pallas kernels: 84.2 us -> 67.1 us  [line_call(): pl.pallas_call(functools.partial(line_kernel, n, tp, cap, reach, near, na...]
where the time goes in v2:
time: 68.8 us; the launch traced here: 68.6 us
  Pallas kernels  68 us (99%)
    pallas_call x1, Pallas kernels, line_call(): pl.pallas_call(functools.partial(line_kernel, n, tp, cap, reach, near, na...  67.1 us

profile of v2, /device:TPU:0, one launch (start us, length us, event | category | flops | bytes accessed | tf_op | source)
XLA Modules:
  0.0 68.6 jit_solution(8236592544479466300)
XLA Ops:
  0.6 67.1 %line.1 = (bf16[128,2048]{1,0:T(8,128)(2,1)S(1)}, bf16[256,512]{1,0:T(8,128)(2,1)S(1)}) custom-call(bf16[256,2048]{1,0:T(8,128)(2,1)} %refs_0_.1, f32[1,2048]{1,0:T(1,128)} %bitcast.4, s32[2,256]{1,0:T(2,128)} %bitcast.5, f32[2,256]{1,0:T(2,128)} %bitcast.6, bf16[512,256]{1,0:T(8,128)(2,1)} %refs_4_.1, bf16[512,256]{1,0:T(8,128)(2,1)} %refs_5_.1, ...), custom_call_target="tpu_custom_call" | custom-call | tf_op jit(solution)/shard_map/line/pallas_call | solution.py:1447
  67.7 0.9 %settle.1 = (bf16[128,2048]{1,0:T(8,128)(2,1)}, bf16[256,512]{1,0:T(8,128)(2,1)}) custom-call(bf16[128,2048]{1,0:T(8,128)(2,1)S(1)} %get-tuple-element.4.a_ref, bf16[256,512]{1,0:T(8,128)(2,1)S(1)} %get-tuple-element.5.b_ref), custom_call_target="tpu_custom_call" | custom-call | tf_op jit(solution)/shard_map/settle/pallas_call | solution.py:1625

commit v3 on v2

--- a/solution.py
+++ b/solution.py
@@ -685,6 +685,8 @@
     inner = behind >= 1
     longer = jnp.where(stations - 1 - z > z, 1, -1)
 
+    reach_here = jnp.where(inner, near[1], near[0])
+
     def distance(j):
         return jnp.where(j <= 2 * behind, (j + 1) // 2, j - behind)
 
@@ -726,7 +728,8 @@
         name: pltpu.make_async_copy(src, dst, r.load_sem.at[i])
         for i, (name, src, dst) in enumerate(
             [
-                ("moe", r.moe_hbm, r.moe),
+                ("moe", r.moe_hbm.at[pl.ds(0, tokens // 2)], r.moe.at[pl.ds(0, tokens // 2)]),
+                ("more", r.moe_hbm.at[pl.ds(tokens // 2, tokens // 2)], r.moe.at[pl.ds(tokens // 2, tokens // 2)]),
                 ("moe_gain", r.moe_gain_hbm, r.moe_gain),
                 ("ids", r.ids_hbm, r.ids),
                 ("route", r.route_hbm, r.route),
@@ -746,14 +749,31 @@
         if name not in late:
             load.start()
 
-    def own_copy(up, xx):
+    def own_copy(up):
         return remote(
-            r.normed.at[xx * 2 + core],
-            r.tok.at[z, xx],
-            r.own_send.at[up, xx],
-            r.tok_recv.at[z, xx],
+            r.normed.at[mine],
+            r.tok.at[z, chip],
+            r.own_send.at[up],
+            r.tok_recv.at[z, chip],
             ep=(z + 2 * up - 1) * 2 + y,
         )
+
+    half = tokens // 2
+
+    def rest_copy(zz, up, part):
+        span = pl.ds(part * half, half)
+        return remote(
+            r.normed.at[across, span],
+            r.tok.at[zz, 1 - chip, span],
+            r.rest_send.at[up, part],
+            r.rest_recv.at[zz, part],
+            ep=(z + 2 * up - 1) * 2 + y,
+        )
+
+    def passes_rest(j):
+        there = onward(origin(j))
+        wanted = jnp.where((there == 0) | (there == stations - 1), near[0], near[1])
+        return (there >= 0) & (there < stations) & (distance(j) + 1 < wanted)
 
     def own_ids(up):
         return remote(
@@ -870,13 +890,15 @@
             r.mix_x_out.at[span], r.mix_x_in.at[span], r.mix_x_send.at[part], r.mix_x_recv.at[part], tp=across
         )
 
-    loads["moe"].wait()
     loads["moe_gain"].wait()
-    everything = r.moe[...].astype(f32)
-    inverse = lax.rsqrt(jnp.sum(everything * everything, axis=1, keepdims=True) / width + eps_rms)
-    normed_now = (everything * inverse * r.moe_gain[...]).astype(bf16)
-    for part in range(tp):
-        r.normed[part] = normed_now[:, part * quarter : (part + 1) * quarter]
+    for name, begin in (("moe", 0), ("more", tokens // 2)):
+        loads[name].wait()
+        span = pl.ds(begin, tokens // 2)
+        everything = r.moe[span].astype(f32)
+        inverse = lax.rsqrt(jnp.sum(everything * everything, axis=1, keepdims=True) / width + eps_rms)
+        normed_now = (everything * inverse * r.moe_gain[...]).astype(bf16)
+        for part in range(tp):
+            r.normed[part, span] = normed_now[:, part * quarter : (part + 1) * quarter]
     loads["ids"].wait()
     loads["route"].wait()
     r.ids_all[z] = jnp.concatenate([r.ids[...].astype(f32), jnp.zeros((6, tokens), f32)], axis=0)
@@ -901,9 +923,12 @@
             do(1)
 
     each_way(lambda up: own_ids(up).start())
-    each_way(lambda up: own_copy(up, chip).start())
-    if near > 1:
-        each_way(lambda up: own_copy(up, 1 - chip).start())
+    each_way(lambda up: own_copy(up).start())
+    each_way(lambda up: rest_copy(z, up, 0).start())
+
+    @pl.when(jnp.logical_not(inner))
+    def _():
+        each_way(lambda up: rest_copy(z, up, 1).start())
 
     row = lax.broadcasted_iota(jnp.int32, (tokens, tokens), 0)
     col = lax.broadcasted_iota(jnp.int32, (tokens, tokens), 1)
@@ -1041,6 +1066,68 @@
     loads["w_down"].wait()
     expert_step(0, first=True)
 
+    def pull(j):
+        zz = origin(j)
+        there = onward(zz)
+        pass_ids(zz).wait_recv()
+        pass_copy(zz, chip).wait_recv()
+
+        @pl.when((there >= 0) & (there < stations))
+        def _():
+            pass_ids(zz).start()
+            pass_copy(zz, chip).start()
+
+    def pull_rest(j):
+        zz = origin(j)
+        there = onward(zz)
+
+        @pl.when(distance(j) == 1)
+        def _():
+            for part in range(2):
+                rest_copy(zz, 0, part).wait_recv()
+
+        @pl.when(distance(j) > 1)
+        def _():
+            pass_copy(zz, 1 - chip).wait_recv()
+
+        @pl.when(passes_rest(j))
+        def _():
+            pass_copy(zz, 1 - chip).start()
+
+    def spread(j, xx, once):
+        zz = origin(j)
+        rows = jnp.dot(r.picks[j], r.tok[zz, xx], preferred_element_type=f32).astype(bf16)
+        r.side[j, xx] = rows[cap:]
+        r.arrived[xx * 2 + core, block(2 * j), :] = rows[:cap]
+        side_copy(j, xx).start()
+        if once:
+
+            @pl.when(distance(j) >= reach_here)
+            def _():
+                slant_copy(j).start()
+                cross_copy(2 * j).start()
+
+        core_copy(2 * j, xx).start()
+
+    def absorb(j):
+        r.picks[j] = jnp.concatenate(choices(origin(j)), axis=0)
+        spread(j, chip, True)
+
+    def absorb_rest(j):
+        pull_rest(j)
+        spread(j, 1 - chip, False)
+
+    def gather_side(j):
+        for xx in (chip, 1 - chip):
+            side_copy(j, xx).wait_recv()
+            core_copy(2 * j + 1, xx).start()
+
+    def gather_cross(s):
+        @pl.when((distance(s // 2) >= reach_here) & (lax.rem(s, 2) == 0))
+        def _():
+            cross_copy(s).wait_recv()
+            core_copy(s, 1 - chip).start()
+
     loads["ln_gain"].wait()
     loads["w_out"].wait()
     sum_step(0)
@@ -1055,6 +1142,12 @@
     scaled = (r.conv[...] - mean) * lax.rsqrt(variance + eps_norm) * r.ln_gain[...]
     r.act[...] = jax.nn.silu(scaled).astype(bf16)
 
+    @pl.when(inner)
+    def _():
+        pull(1)
+        pull(2)
+        each_way(lambda up: rest_copy(z, up, 1).start())
+
     def mix_part(owner):
         begin = pl.multiple_of(owner * own_rows, own_rows)
         return jnp.dot(r.act[pl.ds(begin, own_rows), :], r.w_out[...], preferred_element_type=f32)
@@ -1071,72 +1164,6 @@
         ).astype(bf16)
     mix_x_copy(0).start()
 
-    def pull(j):
-        zz = origin(j)
-        there = onward(zz)
-        pass_ids(zz).wait_recv()
-        pass_copy(zz, chip).wait_recv()
-
-        @pl.when((there >= 0) & (there < stations))
-        def _():
-            pass_ids(zz).start()
-            pass_copy(zz, chip).start()
-
-    def pull_rest(j):
-        zz = origin(j)
-        there = onward(zz)
-        pass_copy(zz, 1 - chip).wait_recv()
-
-        @pl.when((there >= 0) & (there < stations) & (distance(j) + 1 < near))
-        def _():
-            pass_copy(zz, 1 - chip).start()
-
-    def absorb(j):
-        zz = origin(j)
-        full = distance(j) < near
-
-        @pl.when(full)
-        def _():
-            pull_rest(j)
-
-        ours, theirs = choices(zz)
-        both = jnp.concatenate([ours, theirs], axis=0)
-
-        def spread(xx):
-            rows = jnp.dot(both, r.tok[zz, xx], preferred_element_type=f32).astype(bf16)
-            r.side[j, xx] = rows[cap:]
-            r.arrived[xx * 2 + core, block(2 * j), :] = rows[:cap]
-            side_copy(j, xx).start()
-
-            @pl.when(jnp.logical_not(full))
-            def _():
-                cross_copy(2 * j).start()
-                slant_copy(j).start()
-
-            core_copy(2 * j, xx).start()
-
-        spread(chip)
-
-        @pl.when(full)
-        def _():
-            spread(1 - chip)
-
-    def gather_side(j):
-        for xx in (chip, 1 - chip):
-            side_copy(j, xx).wait_recv()
-            core_copy(2 * j + 1, xx).start()
-
-    def gather_cross(s):
-        @pl.when((distance(s // 2) >= near) & (lax.rem(s, 2) == 0))
-        def _():
-            cross_copy(s).wait_recv()
-            core_copy(s, 1 - chip).start()
-
-    @pl.when(inner)
-    def _():
-        pull(1)
-        pull(2)
-
     plan = schedule(stations)
     early = min(pieces - 1, 2)
 
@@ -1152,6 +1179,8 @@
         b = entry("answer", i)
         c = entry("pull", i)
         d = entry("sum", i)
+        g = entry("rest", i)
+        h = entry("before", i)
         j = a // 2
 
         @pl.when(c >= 0)
@@ -1169,6 +1198,14 @@
         @pl.when((a >= 0) & (lax.rem(a, 2) == 1))
         def _():
             gather_side(j)
+
+        @pl.when((g >= 0) & (distance(g // 2) < reach_here))
+        def _():
+            absorb_rest(g // 2)
+
+        @pl.when(h >= 0)
+        def _():
+            sum_step(h)
 
         @pl.when(e >= 0)
         def _():
@@ -1223,33 +1260,36 @@
         elif k == 1:
             r.total[...] += take(1)
 
+    rest = [s for s in range(2, n) if s % 2 == 0] + [s for s in range(n - 1, 2, -2)]
+    for s in rest[:-2]:
+        r.total[...] += take(s)
     mix_copy(chip).wait_recv()
     mixed = r.mix_own[chip].astype(f32) + r.mix_in[chip].astype(f32)
     for part in range(pieces):
         mix_x_copy(part).wait_recv()
     r.mixer_out[...] = (mixed + r.mix_x_in[...].astype(f32)).astype(bf16)
-    for s in range(2, n - 1):
+    for s in rest[-2:-1]:
         r.total[...] += take(s)
-    r.expert_out[...] = (r.total[...] + take(n - 1)).astype(bf16)
+    r.expert_out[...] = (r.total[...] + take(rest[-1])).astype(bf16)
 
     each_way(lambda up: own_ids(up).wait_send())
-    each_way(lambda up: own_copy(up, chip).wait_send())
-    if near > 1:
-        each_way(lambda up: own_copy(up, 1 - chip).wait_send())
+    each_way(lambda up: own_copy(up).wait_send())
+    each_way(lambda up: rest_copy(z, up, 0).wait_send())
+    each_way(lambda up: rest_copy(z, up, 1).wait_send())
 
     def left(j, _):
         zz = origin(j)
         there = onward(zz)
-        full = distance(j) < near
+        full = distance(j) < reach_here
 
         @pl.when((there >= 0) & (there < stations))
         def _():
             pass_ids(zz).wait_send()
             pass_copy(zz, chip).wait_send()
 
-            @pl.when(distance(j) + 1 < near)
-            def _():
-                pass_copy(zz, 1 - chip).wait_send()
+        @pl.when(passes_rest(j))
+        def _():
+            pass_copy(zz, 1 - chip).wait_send()
 
         side_copy(j, chip).wait_send()
 
@@ -1297,29 +1337,36 @@
     total = 2 * stations
     if stations == 4:
         ends = dict(
-            arrive=[1, 2, 3, 4, 6, 5, -1, 7],
-            expert=[1, 2, 3, 4, -1, 5, 6, 7],
-            sum=[1, 2, 3, -1, 4, 5, 6, 7],
-            answer=[-1, 0, 1, 2, -1, 3, -1, 4],
-            finish=[5, 6, 7],
+            arrive=[1, 2, 4, -1, 6, 3, -1, 7, 5],
+            rest=[-1, -1, -1, 2, -1, -1, 4],
+            expert=[1, -1, -1, 2, -1, 3, 4, 7, 6, 5],
+            sum=[1, -1, -1, 2, -1, 3, 4, 7, 6, 5],
+            answer=[-1, 0, -1, -1, -1, 1, -1, 2, 3, 4],
+            finish=[7, 6, 5],
         )
         mids = dict(
-            arrive=[1, 2, 4, 3, 6, 5, 7],
-            expert=[1, 2, 4, 3, 6, 5, 7],
-            answer=[-1, 0, -1, -1, 4, 1, 6],
-            sum=[1, 2, 4, 3, 6, 5, 7],
+            arrive=[4, 1, 2, 6, 3, 7, 5],
+            rest=[-1, -1, 2, 4],
+            expert=[-1, 1, 2, 4, 3, 7, 6, 5],
+            sum=[-1, 1, -1, 2, 4, 7, 6, 5, 3],
             pull=[-1, -1, -1, 3],
-            finish=[2, 5, 3, 7],
+            answer=[-1, -1, 0, -1, -1, 1, 4, -1, 7],
+            finish=[6, 5, 2, 3],
         )
     else:
         arrive = [1] + list(range(2, total, 2)) + list(range(3, total, 2))
-        ends = dict(arrive=arrive, expert=[1] + [-1] * (total - 2) + list(range(2, total)))
-        ends["finish"] = list(range(total))
+        count = len(arrive)
+        ends = dict(
+            arrive=arrive,
+            rest=[-1] + list(range(2, total, 2)),
+            expert=[1] + [-1] * (count - 1) + list(range(2, total)),
+            finish=list(range(total)),
+        )
         ends["sum"] = ends["expert"]
         mids = dict(ends, pull=[-1] + list(range(3, stations)))
     plan = {}
     steps = max(len(part) for part in list(ends.values()) + list(mids.values()))
-    for name in ("arrive", "expert", "sum", "answer", "pull", "finish"):
+    for name in ("arrive", "rest", "before", "expert", "sum", "answer", "pull", "finish"):
         one, two = ends.get(name, []), mids.get(name, [])
         used = max(len(one), len(two)) if name == "finish" else steps
         plan[name] = [tuple((part + [-1] * used)[k] for part in (one, two)) for k in range(used)]
@@ -1370,14 +1417,17 @@
         w_up=V((width, hidden), bf16),
         w_down=V((hidden, width), bf16),
         w_out=V((chan, out_width), bf16),
-        load_sem=dma((12,)),
+        load_sem=dma((13,)),
         normed=V((tp, tokens, quarter), bf16),
         ids_all=V((stations, 8, tokens), f32),
         above=V((tokens, tokens), bf16),
         tok=V((stations, 2, tokens, quarter), bf16),
         side=V((stations, 2, cap, quarter), bf16),
         arrived=V((tp, n * cap, quarter), bf16),
-        own_send=dma((2, 2)),
+        own_send=dma((2,)),
+        rest_send=dma((2, 2)),
+        rest_recv=dma((stations, 2)),
+        picks=V((stations, 2 * cap, tokens), bf16),
         tok_recv=dma((stations, 2)),
         ids_own_send=dma((2,)),
         ids_recv=dma((stations,)),
@@ -1480,7 +1530,7 @@
     chips = tp // 2
     if chips == 2 and (n // 2) * moe_input.shape[0] <= n * 4 * max(1, moe_input.shape[0] // n):
         return line_call(
-            3,
+            (3, 2),
             glu_value,
             glu_gate,
             conv_kernel,

time: 68.8 us -> 67.7 us (0.984)
  Pallas kernels: 68 us -> 66.2 us
    pallas_call x1, Pallas kernels: 67.1 us -> 65.3 us  [line_call(): pl.pallas_call(functools.partial(line_kernel, n, tp, cap, reach, near, na...]
where the time goes in v3:
time: 67.7 us; the launch traced here: 66.8 us
  Pallas kernels  66.2 us (98%)
    pallas_call x1, Pallas kernels, line_call(): pl.pallas_call(functools.partial(line_kernel, n, tp, cap, reach, near, na...  65.3 us

profile of v3, /device:TPU:0, one launch (start us, length us, event | category | flops | bytes accessed | tf_op | source)
XLA Modules:
  0.0 66.8 jit_solution(5511311453061697403)
XLA Ops:
  0.6 65.3 %line.1 = (bf16[128,2048]{1,0:T(8,128)(2,1)S(1)}, bf16[256,512]{1,0:T(8,128)(2,1)S(1)}) custom-call(bf16[256,2048]{1,0:T(8,128)(2,1)} %refs_0_.1, f32[1,2048]{1,0:T(1,128)} %bitcast.4, s32[2,256]{1,0:T(2,128)} %bitcast.5, f32[2,256]{1,0:T(2,128)} %bitcast.6, bf16[512,256]{1,0:T(8,128)(2,1)} %refs_4_.1, bf16[512,256]{1,0:T(8,128)(2,1)} %refs_5_.1, ...), custom_call_target="tpu_custom_call" | custom-call | tf_op jit(solution)/shard_map/line/pallas_call | solution.py:1497
  65.9 0.9 %settle.1 = (bf16[128,2048]{1,0:T(8,128)(2,1)}, bf16[256,512]{1,0:T(8,128)(2,1)}) custom-call(bf16[128,2048]{1,0:T(8,128)(2,1)S(1)} %get-tuple-element.4.a_ref, bf16[256,512]{1,0:T(8,128)(2,1)S(1)} %get-tuple-element.5.b_ref), custom_call_target="tpu_custom_call" | custom-call | tf_op jit(solution)/shard_map/settle/pallas_call | solution.py:1675
